TPU v7x, 128 devices: a whole 4x4x4 slice. The times are simulated.
128 devices in a mesh: ep: 128 (over z, y, x, core).
Axes of the slice: x: 4, y: 4, z: 4, core: 2. Of those that a mesh axis runs over, the one named last changes fastest.
Arguments:
- tokens: bfloat16 [2304, 2048], P('ep'), may hold values from -6 to 6
- attn_norm_gain: float32 [2048], replicated, may hold values from 0.1 to 1.9
- w_query: bfloat16 [2048, 512], replicated, may hold values from -0.125 to 0.125
- w_key: bfloat16 [2048, 128], replicated, may hold values from -0.125 to 0.125
- w_value: bfloat16 [2048, 128], replicated, may hold values from -0.125 to 0.125
- w_forget: bfloat16 [2048, 8], replicated, may hold values from -0.125 to 0.125
- forget_bias: float32 [8], replicated, may hold values from 0.5 to 4
- w_attn_out: bfloat16 [512, 2048], replicated, may hold values from -0.25 to 0.25
- cache_keys: bfloat16 [2304, 1024, 128], P('ep'), may hold values from -72 to 72
- cache_values: bfloat16 [2304, 1024, 128], P('ep'), may hold values from -6 to 6
- cache_logcum: float32 [2304, 8, 1024], P('ep'), as said below
- cache_lengths: int32 [2304], P('ep'), may hold values from 128 to 1024
- expert_norm_gain: float32 [2048], replicated, may hold values from 0.4 to 40
- expert_ids: int32 [2304, 6], P('ep'), may hold values from 0 to 127, all different within a row; in each aligned block of 18 rows (0 to 17, 18 to 35, ...) at most 2 rows name the same one
- expert_weights: float32 [2304, 6], P('ep'), may hold values from 0.1 to 1
- w_expert_gate: bfloat16 [128, 2048, 512], P('ep'), may hold values from -0.125 to 0.125
- w_expert_up: bfloat16 [128, 2048, 512], P('ep'), may hold values from -0.125 to 0.125
- w_expert_down: bfloat16 [128, 512, 2048], P('ep'), may hold values from -0.25 to 0.25
- w_dense_gate: bfloat16 [2048, 4096], P(None, 'ep'), may hold values from -0.125 to 0.125
- w_dense_up: bfloat16 [2048, 4096], P(None, 'ep'), may hold values from -2 to 2
- w_dense_down: bfloat16 [4096, 2048], P('ep'), may hold values from -0.09375 to 0.09375
- dense_norm_gain: float32 [4096], replicated, may hold values from 0.1 to 1.9
- branch_gate: float32 [2048], replicated, may hold values from -0.125 to 0.125
Outputs:
- result: bfloat16 [2304, 2048], P('ep')
Inputs may be any that keep to these rules, and one draw needn't show every extreme that they name: `cache_logcum`: along the positions of each sequence and head the values never rise. `expert_ids`: each row names 6 different experts; among the rows of one device no expert is named by more than 2 rows, and in every draw some device names some expert exactly 2 times.
All inputs are finite; a program needn't handle non-finite values.
Results may differ from a plain program's by a relative error of at most 0.012.
The roundings to bfloat16 on the way count: a program that leaves them out, or rounds other values in their place, can miss the bound.
Values may be sent and summed in bfloat16 or wider, within the bound.
A program may use at most 128 MiB of HBM per device.

v0:
```python
import jax
import jax.numpy as jnp
from jax import lax
from jax.sharding import PartitionSpec as P

HEADS = 8
KV_HEADS = 2
HEAD_DIM = 64
TOPK = 6


EPS = 1e-06
LIMIT = 7.0
ALPHA = 1.702


def normalize(values, gain):
    return values * lax.rsqrt(jnp.mean(values * values, axis=-1, keepdims=True) + EPS) * gain


def stored(values):
    return lax.optimization_barrier(values.astype(jnp.bfloat16))


def attend(
    query, key_new, value_new, log_forget, cache_keys, cache_values, cache_logcum, cache_lengths
):
    seqs, length = (cache_keys.shape[0], cache_keys.shape[1])
    group = HEADS // KV_HEADS
    scale = HEAD_DIM ** (-0.5)
    heads_q = query.reshape(seqs, KV_HEADS, group, HEAD_DIM)
    keys = cache_keys.reshape(seqs, length, KV_HEADS, HEAD_DIM)
    values = cache_values.reshape(seqs, length, KV_HEADS, HEAD_DIM)
    own_key = key_new.reshape(seqs, KV_HEADS, HEAD_DIM)
    own_value = value_new.astype(jnp.float32).reshape(seqs, KV_HEADS, 1, HEAD_DIM)
    last_index = jnp.broadcast_to((cache_lengths - 1)[:, None, None], (seqs, HEADS, 1))
    carried = jnp.take_along_axis(cache_logcum, last_index, axis=2)[:, :, 0] + log_forget
    offset = (carried[:, :, None] - cache_logcum).reshape(seqs, KV_HEADS, group, length)
    scores = (
        jnp.einsum("skgd,slkd->skgl", heads_q, keys, preferred_element_type=jnp.float32) * scale
        + offset
    )
    live = jnp.arange(length, dtype=jnp.int32)[None, :] < cache_lengths[:, None]
    scores = jnp.where(live[:, None, None, :], scores, -jnp.inf)
    own = jnp.einsum("skgd,skd->skg", heads_q, own_key, preferred_element_type=jnp.float32) * scale
    top = jnp.maximum(jnp.max(scores, axis=-1), own)
    expo = jnp.exp(scores - top[..., None])
    own_expo = jnp.exp(own - top)
    total = jnp.sum(expo, axis=-1) + own_expo
    weights = (expo / total[..., None]).astype(jnp.bfloat16)
    own_weight = stored(own_expo / total).astype(jnp.float32)
    out = jnp.einsum("skgl,slkd->skgd", weights, values, preferred_element_type=jnp.float32)
    out = out + own_weight[..., None] * own_value
    return out.reshape(seqs, HEADS * HEAD_DIM).astype(jnp.bfloat16)


def expert_unit(rows, gate_w, up_w, down_w):
    gate = jnp.minimum(jnp.dot(rows, gate_w, preferred_element_type=jnp.float32), LIMIT)
    up = jnp.clip(jnp.dot(rows, up_w, preferred_element_type=jnp.float32), -LIMIT, LIMIT)
    act = ((up + 1.0) * gate * jax.nn.sigmoid(gate * ALPHA)).astype(jnp.bfloat16)
    return jnp.dot(act, down_w, preferred_element_type=jnp.float32).astype(jnp.bfloat16)


def shards(
    tokens,
    attn_norm_gain,
    w_query,
    w_key,
    w_value,
    w_forget,
    forget_bias,
    w_attn_out,
    cache_keys,
    cache_values,
    cache_logcum,
    cache_lengths,
    expert_norm_gain,
    expert_ids,
    expert_weights,
    w_expert_gate,
    w_expert_up,
    w_expert_down,
    w_dense_gate,
    w_dense_up,
    w_dense_down,
    dense_norm_gain,
    branch_gate,
):
    seqs, width = (tokens.shape[0], tokens.shape[1])
    normed = normalize(tokens.astype(jnp.float32), attn_norm_gain).astype(jnp.bfloat16)
    query = jnp.dot(normed, w_query, preferred_element_type=jnp.float32).astype(jnp.bfloat16)
    key_new = jnp.dot(normed, w_key, preferred_element_type=jnp.float32).astype(jnp.bfloat16)
    value_new = jnp.dot(normed, w_value, preferred_element_type=jnp.float32).astype(jnp.bfloat16)
    log_forget = jax.nn.log_sigmoid(
        jnp.dot(normed, w_forget, preferred_element_type=jnp.float32) + forget_bias
    )
    attended = attend(
        query, key_new, value_new, log_forget, cache_keys, cache_values, cache_logcum, cache_lengths
    )
    mixed = stored(
        tokens.astype(jnp.float32)
        + jnp.dot(attended, w_attn_out, preferred_element_type=jnp.float32)
    )
    routed_in = normalize(mixed.astype(jnp.float32), expert_norm_gain).astype(jnp.bfloat16)
    devices = lax.axis_size("ep")
    experts = devices * w_expert_gate.shape[0]
    capacity = max(2, 2 * seqs * TOPK // experts)
    flat_ids = expert_ids.reshape(-1)
    member = (flat_ids[:, None] == jnp.arange(experts, dtype=jnp.int32)[None, :]).astype(jnp.int32)
    slot = jnp.sum(jnp.cumsum(member, axis=0) * member, axis=1) - 1
    target = flat_ids * capacity + slot
    placement = (
        target[:, None] == jnp.arange(experts * capacity, dtype=jnp.int32)[None, :]
    ).astype(jnp.float32)
    per_token = jnp.sum(placement.reshape(seqs, TOPK, experts * capacity), axis=1).astype(
        jnp.bfloat16
    )
    outgoing = jnp.einsum("sc,sd->cd", per_token, routed_in, preferred_element_type=jnp.float32)
    outgoing = outgoing.astype(jnp.bfloat16).reshape(experts, capacity, width)
    arrived = lax.all_to_all(outgoing, "ep", split_axis=0, concat_axis=0, tiled=True)
    count = arrived.shape[1]
    answer = expert_unit(
        arrived.reshape(-1, width), w_expert_gate[0], w_expert_up[0], w_expert_down[0]
    )
    returned = lax.all_to_all(
        answer.reshape(devices, count, width), "ep", split_axis=0, concat_axis=0, tiled=True
    )
    picked = jnp.dot(
        placement.astype(jnp.bfloat16),
        returned.reshape(experts * capacity, width),
        preferred_element_type=jnp.float32,
    )
    routed = jnp.sum(expert_weights[:, :, None] * picked.reshape(seqs, TOPK, width), axis=1)
    piece = lax.all_gather(routed_in, "ep", axis=0, tiled=True)
    gate_dense = jnp.dot(piece, w_dense_gate, preferred_element_type=jnp.float32)
    up_dense = jnp.dot(piece, w_dense_up, preferred_element_type=jnp.float32)
    units = (jax.nn.silu(gate_dense) * up_dense).astype(jnp.bfloat16)
    own_units = lax.all_to_all(units, "ep", split_axis=0, concat_axis=1, tiled=True).astype(
        jnp.float32
    )
    unit_scale = lax.rsqrt(jnp.mean(own_units * own_units, axis=1, keepdims=True) + EPS)
    hidden = (own_units * unit_scale * dense_norm_gain).astype(jnp.bfloat16)
    dense = jnp.dot(
        hidden,
        lax.all_gather(w_dense_down, "ep", axis=0, tiled=True),
        preferred_element_type=jnp.float32,
    )
    branch_scale = jax.nn.sigmoid(
        jnp.sum(routed_in.astype(jnp.float32) * branch_gate, axis=1, keepdims=True)
    )
    return (mixed.astype(jnp.float32) + routed + branch_scale * dense).astype(jnp.bfloat16)


def solution(mesh):
    in_specs = (
        P("ep", None),
        P(),
        P(),
        P(),
        P(),
        P(),
        P(),
        P(),
        P("ep", None, None),
        P("ep", None, None),
        P("ep", None, None),
        P("ep"),
        P(),
        P("ep", None),
        P("ep", None),
        P("ep", None, None),
        P("ep", None, None),
        P("ep", None, None),
        P(None, "ep"),
        P(None, "ep"),
        P("ep", None),
        P(),
        P(),
    )
    out_specs = P("ep", None)
    return jax.shard_map(shards, mesh=mesh, in_specs=in_specs, out_specs=out_specs, check_vma=False)
```

profile of v0, /device:TPU:0, one launch (start us, length us, event | category | flops | bytes accessed | tf_op | source)
XLA Modules:
  0.0 228.4 jit_solution(16532619259781696633)
XLA Ops:
  9.0 5.5 %gather_fusion = f32[144]{0:T(256)S(1)} fusion(f32[18,8,1024]{2,1,0:T(8,128)} %param.33, s32[144]{0:T(256)S(1)} %reshape.290), kind=kCustom, calls=%fused_computation | custom fusion | bytes 2880 | tf_op jit(solution)/shard_map/jit(take_along_axis)/gather | solution.py:37
  17.4 2.0 convolution_convert_fusion.2
  19.5 6.7 %copy.48 = bf16[18,1024,128]{1,2,0:T(8,128)(2,1)} copy(bf16[18,1024,128]{2,1,0:T(8,128)(2,1)} %param.31) | data formatting | bytes 9437184 | tf_op args[8]
  26.7 3.3 %fusion.80 = (f32[18,2,4]{2,1,0:T(2,128)S(1)}, f32[18,2,4,1024]{3,2,1,0:T(4,128)S(1)}) fusion(f32[18,2,4,1024]{3,2,1,0:T(4,128)S(1)} %reshape.279, bf16[18,2,4,64]{3,2,1,0:T(4,128)(2,1)S(1)} %reshape.277, bf16[18,1024,2,64]{1,3,2,0:T(8,128)(2,1)} %bitcast.60, pred[18,1024]{1,0:T(8,128)(4,1)S(1)} %iota_compare_fusion.2), kind=kOutput, calls=%fused_computation.112 | convolution fusion | flops 19464048 | bytes 5935680 | tf_op jit(solution)/shard_map/skgd,slkd->skgl/dot_general | solution.py:40
  30.8 6.6 %copy.52 = bf16[18,1024,128]{1,2,0:T(8,128)(2,1)} copy(bf16[18,1024,128]{2,1,0:T(8,128)(2,1)} %param.32) | data formatting | bytes 9437184 | tf_op args[9]
  37.4 3.7 %fusion.31 = bf16[18,2,4,64]{3,2,1,0:T(4,128)(2,1)S(1)} fusion(bf16[18,1024,2,64]{1,3,2,0:T(8,128)(2,1)} %bitcast.61, f32[18,2,4,1024]{3,2,1,0:T(4,128)S(1)} %get-tuple-element.12, f32[18,2,4]{2,1,0:T(2,128)S(1)} %get-tuple-element.8, f32[18,2,4]{2,1,0:T(2,128)S(1)} %multiply_maximum_fusion, f32[18,2,64]{2,1,0:T(2,128)S(1)} %reshape.286, ...), kind=kOutput, calls=%fused_computation.30 | convolution fusion | flops 19344384 | bytes 5337792 | tf_op jit(solution)/shard_map/skgl,slkd->skgd/dot_general | solution.py:52
  41.3 2.0 fusion.2
  46.4 1.5 reshape.282
  48.0 31.0 %all_to_all.23 = bf16[128,2,2048]{2,1,0:T(2,128)(2,1)S(1)} all-to-all(bf16[128,2,2048]{2,1,0:T(2,128)(2,1)} %reshape.282), channel_id=1, replica_groups=mesh['ep'=128] {'ep'}, dimensions={0} | all-to-all | bytes 2097152 | tf_op jit(solution)/shard_map/all_to_all | solution.py:120
  80.2 3.5 %fusion.16 = f32[256,512]{1,0:T(8,128)} fusion(bf16[256,2048]{1,0:T(8,128)(2,1)} %reshape.283, bf16[1,2048,512]{2,1,0:T(8,128)(2,1)} %param.38), kind=kOutput, calls=%fused_computation.24 | convolution fusion | flops 537001984 | bytes 3670016 | tf_op jit(solution)/shard_map/dot_general | solution.py:58
  83.7 4.1 %convolution_convert_fusion = bf16[256,2048]{1,0:T(8,128)(2,1)} fusion(bf16[1,512,2048]{2,1,0:T(8,128)(2,1)S(1)} %copy-done, f32[256,512]{1,0:T(8,128)} %fusion.16, bf16[256,2048]{1,0:T(8,128)(2,1)S(1)} %copy-done.5, bf16[1,2048,512]{2,1,0:T(8,128)(2,1)} %param.39), kind=kOutput, calls=%fused_computation.3 | convolution fusion | flops 1075445760 | bytes 6815744 | tf_op jit(solution)/shard_map/dot_general | solution.py:61
  87.8 2.5 %reshape.284 = bf16[128,2,2048]{2,1,0:T(2,128)(2,1)} reshape(bf16[256,2048]{1,0:T(8,128)(2,1)} %convolution_convert_fusion) | data formatting | bytes 2097152 | tf_op jit(solution)/shard_map/reshape | solution.py:126
  90.4 4.8 %all-to-all-start.1 = ((bf16[128,2,2048]{2,1,0:T(2,128)(2,1)}), bf16[128,2,2048]{2,1,0:T(2,128)(2,1)S(1)}, u32[]{:S(2)}, u32[]{:S(2)}) async-start(bf16[128,2,2048]{2,1,0:T(2,128)(2,1)} %reshape.284), calls=%async_computation.1 | async-start | bytes 2097152 | tf_op jit(solution)/shard_map/all_to_all | solution.py:125
  95.3 22.1 %all-to-all-done.1 = bf16[128,2,2048]{2,1,0:T(2,128)(2,1)S(1)} async-done(((bf16[128,2,2048]{2,1,0:T(2,128)(2,1)}), bf16[128,2,2048]{2,1,0:T(2,128)(2,1)S(1)}, u32[]{:S(2)}, u32[]{:S(2)}) %all-to-all-start.1) | async-done | bytes 1048608 | tf_op jit(solution)/shard_map/all_to_all | solution.py:125
  117.9 12.2 %all-gather.6.cloned.1.call-done = bf16[128,18,2048]{2,1,0:T(8,128)(2,1)} async-done(((bf16[1,18,2048]{2,1,0:T(8,128)(2,1)}), bf16[128,18,2048]{2,1,0:T(8,128)(2,1)}) %all-gather.6.cloned.1.call-update) | async-done | bytes 9437200 | tf_op jit(solution)/shard_map/all_gather | solution.py:134
  130.1 14.1 %reshape.299 = bf16[2304,2048]{1,0:T(8,128)(2,1)} reshape(bf16[128,18,2048]{2,1,0:T(8,128)(2,1)} %all-gather.6.cloned.1.call-done) | data formatting | bytes 18874368
  144.2 6.8 %fusion.82 = f32[2304,32]{0,1:T(8,128)S(1)} fusion(bf16[2304,2048]{1,0:T(8,128)(2,1)} %reshape.299, bf16[2048,32]{0,1:T(8,128)(2,1)S(1)} %copy-done.8), kind=kOutput, calls=%fused_computation.114 | convolution fusion | flops 301989888 | bytes 9863168 | tf_op jit(solution)/shard_map/dot_general | solution.py:135
  151.0 2.9 %fusion = bf16[2304,32]{0,1:T(8,128)(2,1)S(1)} fusion(bf16[2304,2048]{1,0:T(8,128)(2,1)S(1)} %copy-done.3, bf16[2048,32]{0,1:T(8,128)(2,1)S(1)} %copy-done.9, f32[2304,32]{0,1:T(8,128)S(1)} %fusion.82), kind=kOutput, calls=%fused_computation.2 | convolution fusion | flops 302432256 | bytes 10010624 | tf_op jit(solution)/shard_map/dot_general | solution.py:136
  153.9 2.5 %all_to_all.18 = bf16[128,18,32]{1,0,2:T(8,128)(2,1)S(1)} reshape(bf16[2304,32]{0,1:T(8,128)(2,1)S(1)} %fusion) | data formatting | bytes 294912 | tf_op jit(solution)/shard_map/all_to_all | solution.py:138
  156.4 1.5 copy.56
  159.2 6.8 %all-to-all-start.2 = ((bf16[128,2,288]{2,1,0:T(2,128)(2,1)}), bf16[128,2,288]{2,1,0:T(2,128)(2,1)S(1)}, u32[]{:S(2)}, u32[]{:S(2)}) async-start(bf16[128,2,288]{2,1,0:T(2,128)(2,1)} %reshape.306), calls=%async_computation.2 | async-start | bytes 393216 | tf_op jit(solution)/shard_map/all_to_all | solution.py:138
  166.6 10.2 %all-to-all-done.2 = bf16[128,2,288]{2,1,0:T(2,128)(2,1)S(1)} async-done(((bf16[128,2,288]{2,1,0:T(2,128)(2,1)}), bf16[128,2,288]{2,1,0:T(2,128)(2,1)S(1)}, u32[]{:S(2)}, u32[]{:S(2)}) %all-to-all-start.2) | async-done | bytes 147488 | tf_op jit(solution)/shard_map/all_to_all | solution.py:138
  178.6 34.1 %all-gather.4.cloned.1.call-done = bf16[4096,2048]{1,0:T(8,128)(2,1)} async-done(((bf16[32,2048]{1,0:T(8,128)(2,1)}), bf16[4096,2048]{1,0:T(8,128)(2,1)}) %all-gather.4.cloned.1.call-update) | async-done | bytes 16777232 | tf_op jit(solution)/shard_map/all_gather | solution.py:145
  212.7 8.9 %fusion.3 = bf16[18,2048]{1,0:T(8,128)(2,1)} fusion(bf16[4096,2048]{1,0:T(8,128)(2,1)} %all-gather.4.cloned.1.call-done, f32[18,2048]{1,0:T(8,128)S(1)} %fusion.10, bf16[18,2048]{1,0:T(8,128)(2,1)S(1)} %fusion.2, f32[18,4096]{1,0:T(8,128)S(1)} %reshape.287, f32[4096]{0:T(1024)S(1)} %copy-done.11, f32[18]{0:T(128)S(1)} %add_rsqrt_fusion, ...), kind=kOutput, calls=%fused_computation.10 | convolution fusion | flops 302395392 | bytes 17383568 | tf_op jit(solution)/shard_map/dot_general | solution.py:143
  (94 shorter events, 15.2 us)
Async XLA Ops:
  6.5 77.2 %copy-start = (bf16[1,512,2048]{2,1,0:T(8,128)(2,1)S(1)}, bf16[1,512,2048]{2,1,0:T(8,128)(2,1)}, u32[]{:S(2)}) copy-start(bf16[1,512,2048]{2,1,0:T(8,128)(2,1)} %param.40) | copy-start | bytes 6291460
  6.5 123.5 %all-gather.6.cloned.1.call-start = ((), (), s32[]{:S(2)}) async-start(), calls=%async_computation.4 | async-start | bytes 12681216 | tf_op jit(solution)/shard_map/all_gather | solution.py:134
  9.0 5.7 %copy-start.4 = (bf16[18,2048]{1,0:T(8,128)(2,1)S(1)}, bf16[18,2048]{1,0:T(8,128)(2,1)}, u32[]{:S(2)}) copy-start(bf16[18,2048]{1,0:T(8,128)(2,1)} %param.23) | copy-start | bytes 221188
  9.0 5.8 %copy-start.10 = (f32[2048]{0:T(1024)S(1)}, f32[2048]{0:T(1024)}, u32[]{:S(2)}) copy-start(f32[2048]{0:T(1024)} %param.24) | copy-start | bytes 24580
  9.0 5.8 %copy-start.16 = (bf16[2048,8]{0,1:T(8,128)(2,1)S(1)}, bf16[2048,8]{0,1:T(8,128)(2,1)}, u32[]{:S(2)}) copy-start(bf16[2048,8]{0,1:T(8,128)(2,1)} %param.28) | copy-start | bytes 98308
  9.0 5.8 %copy-start.17 = (f32[8]{0:T(128)S(1)}, f32[8]{0:T(128)}, u32[]{:S(2)}) copy-start(f32[8]{0:T(128)} %param.29) | copy-start | bytes 100
  9.0 6.2 %copy-start.2 = (f32[18,8,1024]{2,1,0:T(8,128)S(1)}, f32[18,8,1024]{2,1,0:T(8,128)}, u32[]{:S(2)}) copy-start(f32[18,8,1024]{2,1,0:T(8,128)} %param.33) | copy-start | bytes 1769476
  19.5 6.7 %copy-start.6 = (bf16[2048,128]{1,0:T(8,128)(2,1)S(1)}, bf16[2048,128]{1,0:T(8,128)(2,1)}, u32[]{:S(2)}) copy-start(bf16[2048,128]{1,0:T(8,128)(2,1)} %param.26) | copy-start | bytes 1572868
  26.7 3.7 %copy-start.7 = (bf16[2048,128]{1,0:T(8,128)(2,1)S(1)}, bf16[2048,128]{1,0:T(8,128)(2,1)}, u32[]{:S(2)}) copy-start(bf16[2048,128]{1,0:T(8,128)(2,1)} %param.27) | copy-start | bytes 1572868
  41.1 2.3 copy-start.12
  41.1 2.3 copy-start.13
  41.2 3.9 %copy-start.14 = (s32[18,6]{0,1:T(8,128)S(1)}, s32[18,6]{0,1:T(8,128)}, u32[]{:S(2)}) copy-start(s32[18,6]{0,1:T(8,128)} %param.36) | copy-start | bytes 1300
  44.3 168.4 %all-gather.4.cloned.1.call-start = ((), (), s32[]{:S(2)}) async-start(), calls=%async_computation.3 | async-start | bytes 16908288 | tf_op jit(solution)/shard_map/all_gather | solution.py:145
  80.2 3.5 %copy-start.5 = (bf16[256,2048]{1,0:T(8,128)(2,1)S(1)}, bf16[256,2048]{1,0:T(8,128)(2,1)}, u32[]{:S(2)}) copy-start(bf16[256,2048]{1,0:T(8,128)(2,1)} %reshape.283) | copy-start | bytes 3145732
  87.8 7.4 %copy-start.15 = (f32[18,6]{0,1:T(8,128)S(1)}, f32[18,6]{0,1:T(8,128)}, u32[]{:S(2)}) copy-start(f32[18,6]{0,1:T(8,128)} %param.37) | copy-start | bytes 1300
  90.4 27.1 %all-to-all-start.1 = ((bf16[128,2,2048]{2,1,0:T(2,128)(2,1)}), bf16[128,2,2048]{2,1,0:T(2,128)(2,1)S(1)}, u32[]{:S(2)}, u32[]{:S(2)}) async-start(bf16[128,2,2048]{2,1,0:T(2,128)(2,1)} %reshape.284), calls=%async_computation.1 | async-start | bytes 2097152 | tf_op jit(solution)/shard_map/all_to_all | solution.py:125
  117.9 26.3 %copy-start.8 = (bf16[2048,32]{0,1:T(8,128)(2,1)S(1)}, bf16[2048,32]{0,1:T(8,128)(2,1)}, u32[]{:S(2)}) copy-start(bf16[2048,32]{0,1:T(8,128)(2,1)} %param.41) | copy-start | bytes 393220
  144.2 6.8 %copy-start.3 = (bf16[2304,2048]{1,0:T(8,128)(2,1)S(1)}, bf16[2304,2048]{1,0:T(8,128)(2,1)}, u32[]{:S(2)}) copy-start(bf16[2304,2048]{1,0:T(8,128)(2,1)} %reshape.299) | copy-start | bytes 28311556
  144.2 6.8 %copy-start.9 = (bf16[2048,32]{0,1:T(8,128)(2,1)S(1)}, bf16[2048,32]{0,1:T(8,128)(2,1)}, u32[]{:S(2)}) copy-start(bf16[2048,32]{0,1:T(8,128)(2,1)} %param.42) | copy-start | bytes 393220
  159.2 17.6 %all-to-all-start.2 = ((bf16[128,2,288]{2,1,0:T(2,128)(2,1)}), bf16[128,2,288]{2,1,0:T(2,128)(2,1)S(1)}, u32[]{:S(2)}, u32[]{:S(2)}) async-start(bf16[128,2,288]{2,1,0:T(2,128)(2,1)} %reshape.306), calls=%async_computation.2 | async-start | bytes 393216 | tf_op jit(solution)/shard_map/all_to_all | solution.py:138
  177.4 35.3 %copy-start.11 = (f32[4096]{0:T(1024)S(1)}, f32[4096]{0:T(1024)}, u32[]{:S(2)}) copy-start(f32[4096]{0:T(1024)} %param.44) | copy-start | bytes 49156
  212.7 8.9 %copy-start.1 = (bf16[1,512,2048]{2,1,0:T(8,128)(2,1)S(1)}, bf16[1,512,2048]{2,1,0:T(8,128)(2,1)}, u32[]{:S(2)}) copy-start(bf16[1,512,2048]{2,1,0:T(8,128)(2,1)} %param.40) | copy-start | bytes 6291460
Sparse Core Ops, SparseCore 0:
  44.4 85.5 all-gather.5
  133.2 79.4 all-gather.3
where the time goes:
time: 231 us; the launch traced here: 228 us
  waiting for transfers between devices  79.3 us (34%)
  local copies, waits for them, and re-layouts  47.7 us (21%)
  matrix products  39.1 us (17%)
  blocking collectives  31 us (13%)
  between operations  13.8 us (6%)
  starting transfers between devices  11.7 us (5%)
  other arithmetic  5.76 us (2%)
    all_gather x1, waiting for transfers between devices, shards(): lax.all_gather(w_dense_down, 'ep', axis=0, tiled=True)  34.1 us
    all_to_all x1, blocking collectives, shards(): lax.all_to_all(outgoing, 'ep', split_axis=0, concat_axis=0, tiled=True)  31 us
    unnamed x45, local copies, waits for them, and re-layouts  29.5 us
    all_to_all x1, waiting for transfers between devices, shards(): lax.all_to_all(answer.reshape(devices, count, width), 'ep', split_axis=0,...  22.1 us
    all_gather x1, waiting for transfers between devices, shards(): piece = lax.all_gather(routed_in, 'ep', axis=0, tiled=True)  12.2 us
    all_to_all x1, waiting for transfers between devices, shards(): lax.all_to_all(units, 'ep', split_axis=0, concat_axis=1, tiled=True)  10.2 us
    dot_general x1, matrix products, shards(): jnp.dot(hidden, lax.all_gather(w_dense_down, 'ep', axis=0, tiled=True), p...  8.89 us
    all_to_all x1, starting transfers between devices, shards(): lax.all_to_all(units, 'ep', split_axis=0, concat_axis=1, tiled=True)  6.81 us
  transfers between devices with their start and end apart: 4, of which 4 were waited for; matrix products, arithmetic and copies ran while one was open for 19% of the time, Pallas kernels for 0%

commit v1 on v0

v1 whole, which is shorter than its diff:
```python
import jax
import jax.numpy as jnp
from jax import lax
from jax.experimental import pallas as pl
from jax.experimental.pallas import tpu as pltpu
from jax.sharding import PartitionSpec as P

MESH = pl.DeviceIdType.MESH
F32 = jnp.float32
BF16 = jnp.bfloat16

N = 128
T = 18
D = 2048
KT = 16
LEN = 1024
HEADS = 8
FF = 512
UNITS = 32
GROUP = 16
GU = 256
EPS = 1e-06
LIMIT = 7.0
ALPHA = 1.702
SEQ_STEP = 6

NT = (((1,), (1,)), ((), ()))


def dot(a, b):
    return jnp.dot(a, b, preferred_element_type=F32)


def dot_nt(a, b):
    return lax.dot_general(a, b, NT, preferred_element_type=F32)


def iota(shape, dim):
    return lax.broadcasted_iota(jnp.int32, shape, dim)


def normalize(values, gain):
    mean = jnp.mean(values * values, axis=-1, keepdims=True)
    return values * lax.rsqrt(mean + EPS) * gain


def onehot(mask):
    return jnp.where(mask, 1.0, 0.0).astype(BF16)


def kernel(
    lens,
    tokens,
    attn_gain,
    wf_t,
    forget_bias,
    expert_gain,
    ids_t,
    ew_t,
    dense_gain,
    branch_gate,
    wq_h,
    wk_h,
    wv_h,
    wo_h,
    ck_h,
    cv_h,
    cl_h,
    weg_h,
    weu_h,
    wed_h,
    wdg_h,
    wdu_h,
    wdd_h,
    out,
    bounce_x,
    bounce_y,
    bounce_r,
    bounce_p,
    wq,
    wk,
    wv,
    wo,
    ck,
    cv,
    cl,
    weg,
    weu,
    wed,
    wgu,
    wdd,
    qs,
    os,
    mixed,
    xs,
    xr,
    ys,
    yr,
    rk,
    rp,
    ps,
    rr,
    ssv,
    ssr,
    w_sem,
    kv_sem,
    own_sem,
    gs_sem,
    gr_sem,
    fs_sem,
    fr_sem,
    a_sem,
):
    me = lax.axis_index("ep")
    z = me // 32
    p = lax.rem(me, 32)
    q = p // 2
    c = lax.rem(p, 2)
    block = z * 2 + c

    barrier = pltpu.get_barrier_semaphore()

    def greet(i, carry):
        pl.semaphore_signal(
            barrier, inc=1, device_id=(lax.rem(me + i, N),), device_id_type=MESH
        )
        return carry

    lax.fori_loop(1, N, greet, 0)

    def fetch(src, dst, sem):
        return pltpu.make_async_copy(src, dst, sem)

    first = [
        fetch(wq_h, wq, w_sem.at[0]),
        fetch(wk_h, wk, w_sem.at[1]),
        fetch(wv_h, wv, w_sem.at[2]),
    ]
    for copy in first:
        copy.start()

    def caches(s):
        return (
            fetch(ck_h.at[s], ck.at[s], kv_sem.at[0, s]),
            fetch(cl_h.at[s], cl.at[s], kv_sem.at[1, s]),
            fetch(cv_h.at[s], cv.at[s], kv_sem.at[2, s]),
        )

    def start_cache(s, carry):
        for copy in caches(s):
            copy.start()
        return carry

    lax.fori_loop(0, T, start_cache, 0)
    rows_b = pl.ds(pl.multiple_of(block * UNITS, UNITS), UNITS)
    rows_u = pl.ds(pl.multiple_of(GU + block * UNITS, UNITS), UNITS)
    late = [
        fetch(wo_h, wo, w_sem.at[3]),
        fetch(wdg_h, wgu.at[rows_b], w_sem.at[4]),
        fetch(wdu_h, wgu.at[rows_u], w_sem.at[5]),
        fetch(wdd_h, wdd.at[rows_b], w_sem.at[6]),
        fetch(weg_h.at[0], weg, w_sem.at[7]),
        fetch(weu_h.at[0], weu, w_sem.at[8]),
        fetch(wed_h.at[0], wed, w_sem.at[9]),
    ]
    for copy in late:
        copy.start()

    expert = iota((N, T), 0)
    member = jnp.zeros((N, T), F32)
    weight = jnp.zeros((N, T), F32)
    for k in range(6):
        named = ids_t[k : k + 1, :] == expert
        member = jnp.where(named, 1.0, member)
        weight = jnp.where(named, ew_t[k : k + 1, :], weight)
    upper = onehot(iota((T, T), 0) <= iota((T, T), 1))
    order = dot(member.astype(BF16), upper)
    rank = [
        jnp.where((order == r + 1.0) & (member > 0.5), 1.0, 0.0) for r in range(2)
    ]
    spread = [onehot(iota((2 * N, N), 0) == 2 * iota((2 * N, N), 1) + r) for r in range(2)]
    place = sum(dot(spread[r], rank[r].astype(BF16)) for r in range(2)).astype(BF16)
    eye = onehot(iota((24, T), 0) == iota((24, T), 1))
    parts = []
    rest = weight
    for _ in range(3):
        part = rest.astype(BF16)
        rest = rest - part.astype(F32)
        laid = sum(
            dot(spread[r], (part.astype(F32) * rank[r]).astype(BF16)) for r in range(2)
        )
        parts.append(dot_nt(eye, laid.astype(BF16)).astype(BF16))
    combine = jnp.concatenate(parts, axis=0)

    tok = tokens[...].astype(F32)
    normed = normalize(tok, attn_gain[...]).astype(BF16)
    for copy in first:
        copy.wait()
    query = dot(normed, wq[...]).astype(BF16).astype(F32)
    key_new = dot(normed, wk[...]).astype(BF16).astype(F32)
    value_new = dot(normed, wv[...]).astype(BF16).astype(F32)
    bias = jnp.sum(
        jnp.where(iota((8, 8), 0) == iota((8, 8), 1), forget_bias[...], 0.0),
        axis=1,
        keepdims=True,
    )
    raw = dot_nt(wf_t[...], normed) + bias
    log_forget = jnp.minimum(raw, 0.0) - jnp.log1p(jnp.exp(-jnp.abs(raw)))
    low = iota((T, 128), 1) < 64
    for h in range(HEADS):
        tile = query[:, (h // 2) * 128 : (h // 2 + 1) * 128]
        if (h % 2) != (h // 4):
            tile = pltpu.roll(tile, 64, 1)
        qs[:, h, :] = jnp.where(low if h < 4 else ~low, tile, 0.0)
    key_mask = iota((T, 128), 0)
    head_lane = iota((8, T), 1)
    position = iota((8, LEN), 1)

    def sequence(s):
        for copy in caches(s):
            copy.wait()
        qb = qs[s]
        k_row = jnp.sum(jnp.where(key_mask == s, key_new, 0.0), axis=0, keepdims=True)
        v_row = jnp.sum(jnp.where(key_mask == s, value_new, 0.0), axis=0, keepdims=True)
        own = jnp.sum(qb * k_row, axis=1, keepdims=True) * 0.125
        forget = jnp.sum(jnp.where(head_lane == s, log_forget, 0.0), axis=1, keepdims=True)
        logcum = cl[s]
        length = lens[s]
        last = jnp.sum(
            jnp.where(position == length - 1, logcum, 0.0), axis=1, keepdims=True
        )
        carried = last + forget
        scores = dot_nt(qb.astype(BF16), ck[s]) * 0.125 + (carried - logcum)
        scores = jnp.where(position < length, scores, -jnp.inf)
        top = jnp.maximum(jnp.max(scores, axis=1, keepdims=True), own)
        expo = jnp.exp(scores - top)
        own_expo = jnp.exp(own - top)
        scale = 1.0 / (jnp.sum(expo, axis=1, keepdims=True) + own_expo)
        weights = (expo * scale).astype(BF16)
        own_weight = (own_expo * scale).astype(BF16).astype(F32)
        os[s] = dot(weights, cv[s]) + own_weight * v_row

    def sequences(g, carry):
        for i in range(SEQ_STEP):
            sequence(g * SEQ_STEP + i)
        return carry

    sequences(0, 0)

    pl.semaphore_wait(barrier, N - 1)
    for copy in late[1:4]:
        copy.wait()

    def dense_weights(rows, rows_up, i, peer):
        return [
            pltpu.make_async_remote_copy(
                src_ref=ref.at[r],
                dst_ref=ref.at[r],
                send_sem=gs_sem.at[i, j],
                recv_sem=gr_sem.at[i, j],
                device_id=(peer,),
                device_id_type=MESH,
            )
            for j, (ref, r) in enumerate(((wgu, rows), (wgu, rows_up), (wdd, rows)))
        ]

    def block_rows(b):
        return (
            pl.ds(pl.multiple_of(b * UNITS, UNITS), UNITS),
            pl.ds(pl.multiple_of(GU + b * UNITS, UNITS), UNITS),
        )

    for i in range(1, 4):
        for copy in dense_weights(rows_b, rows_u, i, lax.rem(me + 32 * i, N)):
            copy.start()
    partner = me + 1 - 2 * c
    for copy in dense_weights(rows_b, rows_u, 4, partner):
        copy.start()

    lax.fori_loop(1, T // SEQ_STEP, sequences, 0)

    late[0].wait()
    tiles = []
    for t in range(4):
        even, odd = os[:, 2 * t, :], os[:, 2 * t + 1, :]
        if t < 2:
            odd = pltpu.roll(odd, 64, 1)
        else:
            even = pltpu.roll(even, 64, 1)
        tiles.append(jnp.where(low, even, odd))
    attended = jnp.concatenate(tiles, axis=1).astype(BF16)
    mixed[...] = (tok + dot(attended, wo[...])).astype(BF16)
    routed_in = normalize(mixed[...].astype(F32), expert_gain[...]).astype(BF16)
    branch = jax.nn.sigmoid(
        jnp.sum(routed_in.astype(F32) * branch_gate[...], axis=1, keepdims=True)
    )

    for k in range(KT):
        rk[k] = routed_in[:, k * 128 : (k + 1) * 128]
    for n in range(4):
        cols = slice(n * 512, (n + 1) * 512)
        sent = dot(place, routed_in[:, cols]).astype(BF16)
        for k in range(4):
            xs[n * 4 + k] = sent[:, k * 128 : (k + 1) * 128]

    def pair(ref, d):
        return ref.at[:, pl.ds(2 * d, 2), :]

    def exchange(src, dst, i):
        def body(j, carry):
            d = lax.rem(me + j, N)
            pltpu.make_async_remote_copy(
                src_ref=pair(src, d),
                dst_ref=pair(dst, me),
                send_sem=fs_sem.at[i],
                recv_sem=fr_sem.at[i],
                device_id=(d,),
                device_id_type=MESH,
            ).start()
            return carry

        lax.fori_loop(1, N, body, 0)

    def exchanged(src, dst, i):
        return pltpu.make_async_remote_copy(
            src_ref=src.at[:, pl.ds(0, 2 * (N - 1)), :],
            dst_ref=dst.at[:, pl.ds(0, 2 * (N - 1)), :],
            send_sem=fs_sem.at[i],
            recv_sem=fr_sem.at[i],
            device_id=(lax.rem(me + 1, N),),
            device_id_type=MESH,
        )

    def triple(ref, b):
        return ref.at[:, pl.ds(T * b, T), :]

    def mate(i):
        return z * 32 + lax.rem(q + i, GROUP) * 2 + c

    def group_wait(ref, i):
        part = ref.at[:, pl.ds(0, T * (GROUP - 1)), :]
        return pltpu.make_async_remote_copy(
            src_ref=part,
            dst_ref=part,
            send_sem=fs_sem.at[i],
            recv_sem=fr_sem.at[i],
            device_id=(mate(1),),
            device_id_type=MESH,
        )

    exchange(xs, xr, 0)
    own_x = fetch(pair(xs, me), bounce_x, own_sem.at[0])
    own_r = fetch(rk, bounce_r, own_sem.at[1])
    own_x.start()
    own_r.start()
    for i in range(1, GROUP):
        pltpu.make_async_remote_copy(
            src_ref=rk,
            dst_ref=triple(rp, q),
            send_sem=fs_sem.at[2],
            recv_sem=fr_sem.at[2],
            device_id=(mate(i),),
            device_id_type=MESH,
        ).start()
    own_x.wait()
    own_r.wait()
    own_x = fetch(bounce_x, pair(xr, me), own_sem.at[0])
    own_r = fetch(bounce_r, triple(rp, q), own_sem.at[1])
    own_x.start()
    own_r.start()

    for i in range(1, 4):
        theirs = block_rows(lax.rem(z + 4 - i, 4) * 2 + c)
        for copy in dense_weights(*theirs, i, partner):
            copy.wait_recv()
        for copy in dense_weights(*theirs, 4 + i, partner):
            copy.start()

    for copy in late[4:]:
        copy.wait()
    own_x.wait()
    exchanged(xs, xr, 0).wait_recv()
    for m in range(2):
        rows = slice(m * 128, (m + 1) * 128)
        x = jnp.concatenate([xr[k, rows, :] for k in range(KT)], axis=1)
        gate = jnp.minimum(dot(x, weg[...]), LIMIT)
        up = jnp.clip(dot(x, weu[...]), -LIMIT, LIMIT)
        act = ((up + 1.0) * gate * jax.nn.sigmoid(gate * ALPHA)).astype(BF16)
        for n in range(4):
            answer = dot(act, wed[:, n * 512 : (n + 1) * 512]).astype(BF16)
            for k in range(4):
                ys[n * 4 + k, rows, :] = answer[:, k * 128 : (k + 1) * 128]
    exchange(ys, yr, 1)
    own_y = fetch(pair(ys, me), bounce_y, own_sem.at[0])
    own_y.start()
    own_y.wait()
    own_y = fetch(bounce_y, pair(yr, me), own_sem.at[0])
    own_y.start()

    lane = iota((1, 128), 1)
    gains = []
    for j in range(4):
        row = dense_gain[pl.ds(j * 8 + q // 2, 1), :]
        odd = jnp.full((1, 128), lax.rem(q, 2), jnp.int32) == 1
        gains.append(jnp.where(odd, pltpu.roll(row, 64, 1), row))
    gain = jnp.concatenate(
        [
            jnp.where(lane < 64, gains[2 * j], pltpu.roll(gains[2 * j + 1], 64, 1))
            for j in range(2)
        ],
        axis=1,
    )
    for copy in dense_weights(*block_rows(z * 2 + 1 - c), 4, partner):
        copy.wait_recv()
    for i in range(1, 4):
        theirs = block_rows(lax.rem(z + 4 - i, 4) * 2 + 1 - c)
        for copy in dense_weights(*theirs, 4 + i, partner):
            copy.wait_recv()
    own_r.wait()
    group_wait(rp, 2).wait_recv()
    ones = jnp.ones((8, GU), BF16)
    ssv[...] = jnp.zeros_like(ssv)
    for m in range(3):
        rows = slice(m * 96, (m + 1) * 96)
        r = jnp.concatenate([rp[k, rows, :] for k in range(KT)], axis=1)
        both = dot_nt(r, wgu[...])
        gate, up = both[:, :GU], both[:, GU:]
        units = (gate * jax.nn.sigmoid(gate) * up).astype(BF16).astype(F32)
        square = units * units
        high = square.astype(BF16)
        rest = (square - high.astype(F32)).astype(BF16)
        total = dot_nt(ones, high) + dot_nt(ones, rest)
        ssv[:, m * 128 : m * 128 + 96] = total[0:1, :]
        hidden = (units * gain).astype(BF16)
        for n in range(4):
            part = dot(hidden, wdd[:, n * 512 : (n + 1) * 512]).astype(BF16)
            for k in range(4):
                ps[n * 4 + k, rows, :] = part[:, k * 128 : (k + 1) * 128]

    def sums(i):
        return pltpu.make_async_remote_copy(
            src_ref=ssv,
            dst_ref=ssr.at[q],
            send_sem=fs_sem.at[4],
            recv_sem=fr_sem.at[4],
            device_id=(mate(i),),
            device_id_type=MESH,
        )

    for i in range(1, GROUP):
        other = lax.rem(q + i, GROUP)
        pltpu.make_async_remote_copy(
            src_ref=triple(ps, other),
            dst_ref=triple(rr, q),
            send_sem=fs_sem.at[3],
            recv_sem=fr_sem.at[3],
            device_id=(mate(i),),
            device_id_type=MESH,
        ).start()
        sums(i).start()
    own_p = fetch(triple(ps, q), bounce_p, own_sem.at[1])
    own_p.start()
    ssr[q] = ssv[...]
    own_p.wait()
    own_p = fetch(bounce_p, triple(rr, q), own_sem.at[1])
    own_p.start()

    own_y.wait()
    exchanged(ys, yr, 1).wait_recv()
    own_p.wait()
    group_wait(rr, 3).wait_recv()
    some = ssr.at[pl.ds(0, GROUP - 1)]
    sum_wait = pltpu.make_async_remote_copy(
        src_ref=some,
        dst_ref=some,
        send_sem=fs_sem.at[4],
        recv_sem=fr_sem.at[4],
        device_id=(mate(1),),
        device_id_type=MESH,
    )
    sum_wait.wait_recv()
    total = ssr[0]
    for i in range(1, GROUP):
        total = total + ssr[i]
    spot = T * q + iota((T, 384), 0)
    spot = spot + (spot // 96) * 32
    squares = jnp.sum(
        jnp.where(iota((T, 384), 1) == spot, total, 0.0), axis=1, keepdims=True
    )
    scale = branch * lax.rsqrt(squares * (1.0 / 4096.0) + EPS)
    gather = onehot(lax.rem(iota((T, T * GROUP), 1), T) == iota((T, T * GROUP), 0))
    for n in range(4):
        y = jnp.concatenate([yr[n * 4 + k] for k in range(4)], axis=1)
        three = dot(combine, y)
        routed = three[0:24] + three[24:48] + three[48:72]
        r = jnp.concatenate([rr[n * 4 + k] for k in range(4)], axis=1)
        dense = dot(gather, r)
        cols = slice(n * 512, (n + 1) * 512)
        out[:, cols] = (
            mixed[:, cols].astype(F32) + routed[0:T] + scale * dense
        ).astype(BF16)

    exchanged(xs, xr, 0).wait_send()
    exchanged(ys, yr, 1).wait_send()
    group_wait(rp, 2).wait_send()
    group_wait(rr, 3).wait_send()
    sum_wait.wait_send()
    for i in range(1, 8):
        for copy in dense_weights(rows_b, rows_u, i, partner):
            copy.wait_send()


def shards(
    tokens,
    attn_norm_gain,
    w_query,
    w_key,
    w_value,
    w_forget,
    forget_bias,
    w_attn_out,
    cache_keys,
    cache_values,
    cache_logcum,
    cache_lengths,
    expert_norm_gain,
    expert_ids,
    expert_weights,
    w_expert_gate,
    w_expert_up,
    w_expert_down,
    w_dense_gate,
    w_dense_up,
    w_dense_down,
    dense_norm_gain,
    branch_gate,
):
    vmem = pl.BlockSpec(memory_space=pltpu.VMEM)
    hbm = pl.BlockSpec(memory_space=pl.ANY)
    dma = pltpu.SemaphoreType.DMA
    result = pl.pallas_call(
        kernel,
        out_shape=(
            jax.ShapeDtypeStruct((T, D), BF16),
            jax.ShapeDtypeStruct((KT, 2, 128), BF16),
            jax.ShapeDtypeStruct((KT, 2, 128), BF16),
            jax.ShapeDtypeStruct((KT, T, 128), BF16),
            jax.ShapeDtypeStruct((KT, T, 128), BF16),
        ),
        in_specs=[pl.BlockSpec(memory_space=pltpu.SMEM)] + [vmem] * 9 + [hbm] * 13,
        out_specs=(vmem, hbm, hbm, hbm, hbm),
        scratch_shapes=[
            pltpu.VMEM((D, 512), BF16),
            pltpu.VMEM((D, 128), BF16),
            pltpu.VMEM((D, 128), BF16),
            pltpu.VMEM((512, D), BF16),
            pltpu.VMEM((T, LEN, 128), BF16),
            pltpu.VMEM((T, LEN, 128), BF16),
            pltpu.VMEM((T, HEADS, LEN), F32),
            pltpu.VMEM((D, FF), BF16),
            pltpu.VMEM((D, FF), BF16),
            pltpu.VMEM((FF, D), BF16),
            pltpu.VMEM((2 * GU, D), BF16),
            pltpu.VMEM((GU, D), BF16),
            pltpu.VMEM((T, HEADS, 128), F32),
            pltpu.VMEM((T, HEADS, 128), F32),
            pltpu.VMEM((T, D), BF16),
            pltpu.VMEM((KT, 2 * N, 128), BF16),
            pltpu.VMEM((KT, 2 * N, 128), BF16),
            pltpu.VMEM((KT, 2 * N, 128), BF16),
            pltpu.VMEM((KT, 2 * N, 128), BF16),
            pltpu.VMEM((KT, T, 128), BF16),
            pltpu.VMEM((KT, T * GROUP, 128), BF16),
            pltpu.VMEM((KT, T * GROUP, 128), BF16),
            pltpu.VMEM((KT, T * GROUP, 128), BF16),
            pltpu.VMEM((1, 384), F32),
            pltpu.VMEM((GROUP, 1, 384), F32),
            dma((10,)),
            dma((3, T)),
            dma((2,)),
            dma((8, 3)),
            dma((8, 3)),
            dma((5,)),
            dma((5,)),
            dma((1,)),
        ],
        compiler_params=pltpu.CompilerParams(
            collective_id=0, has_side_effects=True, vmem_limit_bytes=60 << 20
        ),
    )(
        cache_lengths,
        tokens,
        attn_norm_gain.reshape(1, D),
        w_forget.T,
        forget_bias.reshape(1, HEADS),
        expert_norm_gain.reshape(1, D),
        expert_ids.T,
        expert_weights.T,
        dense_norm_gain.reshape(32, 128),
        branch_gate.reshape(1, D),
        w_query,
        w_key,
        w_value,
        w_attn_out,
        cache_keys,
        cache_values,
        cache_logcum,
        w_expert_gate,
        w_expert_up,
        w_expert_down,
        w_dense_gate.T,
        w_dense_up.T,
        w_dense_down,
    )
    return result[0]


def solution(mesh):
    in_specs = (
        P("ep", None),
        P(),
        P(),
        P(),
        P(),
        P(),
        P(),
        P(),
        P("ep", None, None),
        P("ep", None, None),
        P("ep", None, None),
        P("ep"),
        P(),
        P("ep", None),
        P("ep", None),
        P("ep", None, None),
        P("ep", None, None),
        P("ep", None, None),
        P(None, "ep"),
        P(None, "ep"),
        P("ep", None),
        P(),
        P(),
    )
    out_specs = P("ep", None)
    return jax.shard_map(shards, mesh=mesh, in_specs=in_specs, out_specs=out_specs, check_vma=False)
```

time: 231 us -> 79 us (0.34)
  waiting for transfers between devices: 79.3 us -> 0 us
  Pallas kernels: 0 us -> 76.5 us
  local copies, waits for them, and re-layouts: 47.7 us -> 1.54 us
  matrix products: 39.1 us -> 0 us
  blocking collectives: 31 us -> 0 us
  between operations: 13.8 us -> 0.01 us
  starting transfers between devices: 11.7 us -> 0 us
  other arithmetic: 5.76 us -> 0 us
    pallas_call x0 -> x1, Pallas kernels: none -> 76.5 us  [shards(): pl.pallas_call(kernel, out_shape=(jax.ShapeDtypeStruct((T, D), BF16), jax...]
    all_gather x2 -> x0, waiting for transfers between devices: 46.3 us -> none  [the longest x1 34.1 us: shards(): lax.all_gather(w_dense_down, 'ep', axis=0, tiled=True)]
    dot_general x15 -> x0, matrix products: 39.1 us -> none  [the longest x1 8.89 us: shards(): jnp.dot(hidden, lax.all_gather(w_dense_down, 'ep', axis=0, tiled=True), p...]
    all_to_all x2 -> x0, waiting for transfers between devices: 32.3 us -> none  [the longest x1 22.1 us: shards(): lax.all_to_all(answer.reshape(devices, count, width), 'ep', split_axis=0,...]
    all_to_all x1 -> x0, blocking collectives: 31 us -> none  [shards(): lax.all_to_all(outgoing, 'ep', split_axis=0, concat_axis=0, tiled=True)]
    unnamed x45 -> x1, local copies, waits for them, and re-layouts: 29.5 us -> 1.54 us
    all_to_all x2 -> x0, starting transfers between devices: 11.6 us -> none  [the longest x1 6.81 us: shards(): lax.all_to_all(units, 'ep', split_axis=0, concat_axis=1, tiled=True)]
    reshape x7 -> x0, local copies, waits for them, and re-layouts: 7.17 us -> none  [the longest x1 2.55 us: shards(): answer.reshape(devices, count, width)]
  transfers between devices with their start and end apart: 4 -> 0, of which waited for: 4 -> 0; matrix products, arithmetic and copies ran while one was open for 19% -> 0% of each run, Pallas kernels for 0% -> 0%
where the time goes in v1:
time: 79 us; the launch traced here: 78 us
  Pallas kernels  76.5 us (97%)
  local copies, waits for them, and re-layouts  1.54 us (2%)
    pallas_call x1, Pallas kernels, shards(): pl.pallas_call(kernel, out_shape=(jax.ShapeDtypeStruct((T, D), BF16), jax...  76.5 us

profile of v1, /device:TPU:0, one launch (start us, length us, event | category | flops | bytes accessed | tf_op | source)
XLA Modules:
  0.0 78.0 jit_solution(5784230074478830280)
XLA Ops:
  0.0 76.5 %shard_map.217 = (bf16[18,2048]{1,0:T(8,128)(2,1)}, bf16[16,2,128]{2,1,0:T(2,128)(2,1)}, bf16[16,2,128]{2,1,0:T(2,128)(2,1)}, bf16[16,18,128]{2,1,0:T(8,128)(2,1)}, bf16[16,18,128]{2,1,0:T(8,128)(2,1)}) custom-call(s32[18]{0:T(128)} %lens.1, bf16[18,2048]{1,0:T(8,128)(2,1)} %tokens.1, f32[1,2048]{1,0:T(1,128)} %bitcast.14, bf16[8,2048]{1,0:T(8,128)(2,1)} %bitcast.12, ...), custom_call_target="tpu_custom_call" | custom-call | tf_op jit(solution)/shard_map/pallas_call | solution.py:541
  76.5 1.5 %copy.25 = bf16[18,2048]{1,0:T(8,128)(2,1)} copy(bf16[18,2048]{1,0:T(8,128)(2,1)} %get-tuple-element.6) | data formatting | bytes 147456
